TPU v7x, 32 devices: a whole 2x2x4 slice. The times are simulated.
32 devices in a mesh: ep: 4 (over y, x), tp: 8 (over z, core).
Axes of the slice: x: 2, y: 2, z: 4, core: 2. Of those that a mesh axis runs over, the one named last changes fastest.
Arguments:
- query_latent: bfloat16 [2048, 1024], P('ep'), may hold values from -6 to 6
- joint_latent: bfloat16 [2048, 512], P('ep'), may hold values from -6 to 6
- rotary_key: bfloat16 [2048, 32], P('ep'), may hold values from -60 to 60
- query_gain: float32 [1024], replicated, may hold values from 0.1 to 1.9
- joint_gain: float32 [512], replicated, may hold values from 0.1 to 1.9
- query_weight: bfloat16 [1024, 2048], P(None, 'tp'), may hold values from -0.1875 to 0.1875
- query_rotary: bfloat16 [1024, 1024], P(None, 'tp'), may hold values from -0.1875 to 0.1875
- key_weight: bfloat16 [512, 2048], P(None, 'tp'), may hold values from -0.25 to 0.25
- value_weight: bfloat16 [512, 2048], P(None, 'tp'), may hold values from -0.25 to 0.25
- output_weight: bfloat16 [2048, 2048], P('tp'), may hold values from -6 to 6
- expert_input: bfloat16 [2048, 2048], P('ep'), may hold values from -6 to 6
- expert_gain: float32 [2048], replicated, may hold values from 0.1 to 1.9
- routes: int32 [2048, 2], P('ep'), may hold values from 0 to 7, all different within a row; in each aligned block of 512 rows (0 to 511, 512 to 1023, ...) at most 192 rows name the same one
- route_weight: float32 [2048, 2], P('ep'), may hold values from 0.2 to 1
- gate_weight: bfloat16 [8, 2048, 4096], P('ep', None, 'tp'), may hold values from -0.125 to 0.125
- up_weight: bfloat16 [8, 2048, 4096], P('ep', None, 'tp'), may hold values from -0.125 to 0.125
- down_weight: bfloat16 [8, 4096, 2048], P('ep', 'tp'), may hold values from -0.09375 to 0.09375
Outputs:
- mixer_out: bfloat16 [2048, 2048], P(('ep', 'tp'))
- expert_out: bfloat16 [2048, 2048], P('ep', 'tp')
Inputs may be any that keep to these rules, and one draw needn't show every extreme that they name: `routes`: A row names 2 different experts. Among the rows of one device (aligned blocks of 512 rows) no expert is named by more than 192 rows, a bound that some block reaches.
All inputs are finite; a program needn't handle non-finite values.
Results may differ from a plain program's by a relative error of at most 0.019.
The roundings to bfloat16 on the way count: a program that leaves them out, or rounds other values in their place, can miss the bound.
Values may be sent and summed in bfloat16 or wider, within the bound.
A program may use at most 128 MiB of HBM per device.

v0:
```python
import jax
import jax.numpy as jnp
from jax import lax
from jax.sharding import PartitionSpec as P

NOPE = 64
VDIM = 64


NORM_EPSILON = 1e-06
ROTARY_BASE = 10000.0


def norm_rows(source, gain_vector):
    as_float = source.astype(jnp.float32)
    factor = lax.rsqrt(jnp.mean(as_float * as_float, axis=-1, keepdims=True) + NORM_EPSILON)
    return (as_float * factor * gain_vector).astype(jnp.bfloat16)


def rotate(source, positions):
    half_width = source.shape[-1] // 2
    frequencies = ROTARY_BASE ** (-jnp.arange(half_width, dtype=jnp.float32) / half_width)
    angles = positions[:, None] * frequencies[None, :]
    view_shape = (source.shape[0],) + (1,) * (source.ndim - 2) + (half_width,)
    cosine_table = jnp.cos(angles).reshape(view_shape)
    sine_table = jnp.sin(angles).reshape(view_shape)
    first_half = source[..., :half_width]
    second = source[..., half_width:]
    return jnp.concatenate(
        [
            first_half * cosine_table - second * sine_table,
            second * cosine_table + first_half * sine_table,
        ],
        axis=-1,
    )


def attend_block(
    carried, query_plain, query_turned, key_block, value_block, turned_block, score_scale
):
    row_top, row_total, mixed_values = carried
    scores = jnp.einsum("qhd,khd->qhk", query_plain, key_block, preferred_element_type=jnp.float32)
    scores = scores + jnp.einsum(
        "qhd,kd->qhk", query_turned, turned_block, preferred_element_type=jnp.float32
    )
    scores = scores * score_scale
    new_top = jnp.maximum(row_top, jnp.max(scores, axis=-1))
    factor = jnp.exp(row_top - new_top)
    expo = jnp.exp(scores - new_top[..., None])
    row_total = row_total * factor + jnp.sum(expo, axis=-1)
    mixed_values = mixed_values * factor[..., None] + jnp.einsum(
        "qhk,khd->qhd", expo.astype(jnp.bfloat16), value_block, preferred_element_type=jnp.float32
    )
    return (new_top, row_total, mixed_values)


def token_mixer(
    query_latent,
    joint_latent,
    rotary_key,
    query_gain,
    joint_gain,
    query_weight,
    query_rotary,
    key_weight,
    value_weight,
    output_weight,
):
    row_count = query_latent.shape[0]
    head_count = key_weight.shape[1] // NOPE
    turn_width = rotary_key.shape[1]
    offset = lax.axis_index("ep") * row_count
    positions = (offset + jnp.arange(row_count, dtype=jnp.int32)).astype(jnp.float32)
    query_normed = norm_rows(query_latent, query_gain)
    joint_normed = norm_rows(joint_latent, joint_gain)
    turned_key = rotate(rotary_key.astype(jnp.float32), positions).astype(jnp.bfloat16)
    query_plain = jnp.dot(query_normed, query_weight, preferred_element_type=jnp.float32).astype(
        jnp.bfloat16
    )
    query_plain = query_plain.reshape(row_count, head_count, NOPE)
    query_turned = jnp.dot(query_normed, query_rotary, preferred_element_type=jnp.float32)
    query_turned = rotate(
        query_turned.reshape(row_count, head_count, turn_width), positions
    ).astype(jnp.bfloat16)
    score_scale = (NOPE + turn_width) ** (-0.5)
    start_carry = (
        jnp.full((row_count, head_count), -jnp.inf, jnp.float32),
        jnp.zeros((row_count, head_count), jnp.float32),
        jnp.zeros((row_count, head_count, VDIM), jnp.float32),
    )
    key_local = jnp.dot(joint_normed, key_weight, preferred_element_type=jnp.float32).astype(
        jnp.bfloat16
    )
    value_local = jnp.dot(joint_normed, value_weight, preferred_element_type=jnp.float32).astype(
        jnp.bfloat16
    )
    carried = start_carry
    key_piece = lax.all_gather(key_local, "ep", axis=0, tiled=True)
    value_piece = lax.all_gather(value_local, "ep", axis=0, tiled=True)
    turned_piece = lax.all_gather(turned_key, "ep", axis=0, tiled=True)
    block_rows = min(row_count, key_piece.shape[0])
    block_total = key_piece.shape[0] // block_rows

    def scan_step(inner_carry, key_items):
        key_block, value_block, turned_block = key_items
        return (
            attend_block(
                inner_carry,
                query_plain,
                query_turned,
                key_block.reshape(block_rows, head_count, NOPE),
                value_block.reshape(block_rows, head_count, VDIM),
                turned_block,
                score_scale,
            ),
            None,
        )

    carried, _ = lax.scan(
        scan_step,
        carried,
        (
            key_piece.reshape(block_total, block_rows, key_piece.shape[1]),
            value_piece.reshape(block_total, block_rows, value_piece.shape[1]),
            turned_piece.reshape(block_total, block_rows, turn_width),
        ),
    )
    row_top, row_total, mixed_values = carried
    attended = (
        (mixed_values / row_total[..., None])
        .astype(jnp.bfloat16)
        .reshape(row_count, head_count * VDIM)
    )
    return lax.psum_scatter(
        jnp.dot(attended, output_weight, preferred_element_type=jnp.float32).astype(jnp.bfloat16),
        "tp",
        scatter_dimension=0,
        tiled=True,
    )


def experts(expert_input, expert_gain, routes, route_weight, gate_weight, up_weight, down_weight):
    row_count = expert_input.shape[0]
    feature_width = expert_input.shape[1]
    top_count = routes.shape[1]
    group_count = lax.axis_size("ep")
    local_count = gate_weight.shape[0]
    expert_count = local_count * group_count
    capacity = 3 * row_count // (2 * group_count)
    part_width = feature_width // lax.axis_size("tp")
    flat_routes = routes.reshape(-1)
    onehot = (flat_routes[:, None] == jnp.arange(expert_count, dtype=jnp.int32)[None, :]).astype(
        jnp.int32
    )
    rank_within = jnp.sum((jnp.cumsum(onehot, axis=0) - onehot) * onehot, axis=1)
    slot_index = flat_routes * capacity + rank_within
    owner_token = jnp.arange(row_count * top_count, dtype=jnp.int32) // top_count
    slot_token = jnp.zeros((expert_count * capacity,), jnp.int32).at[slot_index].set(owner_token)
    filled = jnp.zeros((expert_count * capacity,), jnp.bfloat16).at[slot_index].set(1.0)
    normed = norm_rows(expert_input, expert_gain)
    outgoing = (normed[slot_token] * filled[:, None]).reshape(
        group_count, local_count, capacity, feature_width
    )
    arrived = lax.all_to_all(outgoing, "ep", split_axis=0, concat_axis=0, tiled=True)
    gate_acts = jnp.einsum(
        "secd,edf->secf", arrived, gate_weight, preferred_element_type=jnp.float32
    )
    up_acts = jnp.einsum("secd,edf->secf", arrived, up_weight, preferred_element_type=jnp.float32)
    hidden = (jax.nn.silu(gate_acts) * up_acts).astype(jnp.bfloat16)
    partial_value = jnp.einsum(
        "secf,efd->secd", hidden, down_weight, preferred_element_type=jnp.float32
    )
    summed = lax.psum_scatter(
        partial_value.astype(jnp.bfloat16), "tp", scatter_dimension=3, tiled=True
    )
    returned = lax.all_to_all(summed, "ep", split_axis=0, concat_axis=0, tiled=True)
    picked = returned.reshape(expert_count * capacity, part_width)[slot_index]
    picked = picked.astype(jnp.float32).reshape(row_count, top_count, part_width)
    return jnp.sum(picked * route_weight[:, :, None], axis=1).astype(jnp.bfloat16)


def local(
    query_latent,
    joint_latent,
    rotary_key,
    query_gain,
    joint_gain,
    query_weight,
    query_rotary,
    key_weight,
    value_weight,
    output_weight,
    expert_input,
    expert_gain,
    routes,
    route_weight,
    gate_weight,
    up_weight,
    down_weight,
):
    mixer_out = token_mixer(
        query_latent,
        joint_latent,
        rotary_key,
        query_gain,
        joint_gain,
        query_weight,
        query_rotary,
        key_weight,
        value_weight,
        output_weight,
    )
    expert_out = experts(
        expert_input, expert_gain, routes, route_weight, gate_weight, up_weight, down_weight
    )
    return (mixer_out, expert_out)


def solution(mesh):
    return jax.shard_map(
        local,
        mesh=mesh,
        in_specs=(
            P("ep", None),
            P("ep", None),
            P("ep", None),
            P(),
            P(),
            P(None, "tp"),
            P(None, "tp"),
            P(None, "tp"),
            P(None, "tp"),
            P("tp", None),
            P("ep", None),
            P(),
            P("ep", None),
            P("ep", None),
            P("ep", None, "tp"),
            P("ep", None, "tp"),
            P("ep", "tp", None),
        ),
        out_specs=(P(("ep", "tp"), None), P("ep", "tp")),
        check_vma=False,
    )
```

profile of v0, /device:TPU:0, one launch (start us, length us, event | category | flops | bytes accessed | tf_op | source)
XLA Modules:
  0.0 264.6 jit_solution(18423690245819720542)
XLA Ops:
  10.0 2.3 reduce-window.6
  13.2 4.3 %scatter_custom_fusion = s32[1536]{0:T(1024)S(1)} fusion(s32[1024]{0:T(1024)S(1)} %bitcast.130, s32[1024]{0:T(1024)S(1)} %add_select_fusion, s32[]{:T(128)} %constant.36.clone.1), kind=kCustom, calls=%fused_computation.89 | custom fusion | bytes 6148 | tf_op jit(solution)/shard_map/scatter | solution.py:158
  19.6 7.6 %scatter_custom_fusion.1 = bf16[1536]{0:T(1024)(128)(2,1)S(1)} fusion(s32[1024]{0:T(1024)S(1)} %bitcast.131, bf16[1024]{0:T(1024)(128)(2,1)S(1)} %broadcast.163, bf16[]{:T(256)} %constant.77.clone.1), kind=kCustom, calls=%fused_computation.93 | custom fusion | bytes 3074 | tf_op jit(solution)/shard_map/scatter | solution.py:159
  27.3 2.1 fusion.22
  29.4 7.1 %gather_fusion = bf16[1536,2048]{1,0:T(8,128)(2,1)} fusion(bf16[512,2048]{1,0:T(8,128)(2,1)S(1)} %fusion.22, s32[2048]{0:T(1024)S(1)} %pad_clamp_fusion), kind=kCustom, calls=%fused_computation | custom fusion | bytes 12589056 | tf_op jit(solution)/shard_map/gather | solution.py:161
  36.5 5.9 %broadcast_multiply_fusion = bf16[4,2,192,2048]{3,2,1,0:T(8,128)(2,1)} fusion(bf16[4,2,192,2048]{3,2,1,0:T(8,128)(2,1)} %bitcast.121, bf16[4,2,192]{2,1,0:T(2,128)(2,1)S(1)} %mul.219), kind=kLoop, calls=%fused_computation.43 | loop fusion | flops 3145728 | bytes 12585984 | tf_op jit(solution)/shard_map/mul | solution.py:161
  42.5 5.4 %all-to-all-start = ((bf16[4,2,192,2048]{3,2,1,0:T(8,128)(2,1)}), bf16[4,2,192,2048]{3,2,1,0:T(8,128)(2,1)}, u32[]{:S(2)}, u32[]{:S(2)}) async-start(bf16[4,2,192,2048]{3,2,1,0:T(8,128)(2,1)} %broadcast_multiply_fusion), calls=%async_computation.1 | async-start | bytes 12582912 | tf_op jit(solution)/shard_map/all_to_all | solution.py:164
  50.6 77.1 %all-to-all-done = bf16[4,2,192,2048]{3,2,1,0:T(8,128)(2,1)} async-done(((bf16[4,2,192,2048]{3,2,1,0:T(8,128)(2,1)}), bf16[4,2,192,2048]{3,2,1,0:T(8,128)(2,1)}, u32[]{:S(2)}, u32[]{:S(2)}) %all-to-all-start) | async-done | bytes 6291488 | tf_op jit(solution)/shard_map/all_to_all | solution.py:164
  127.7 9.1 %fusion.16 = f32[2,4,192,512]{3,2,1,0:T(8,128)} fusion(bf16[4,2,192,2048]{3,2,1,0:T(8,128)(2,1)} %all-to-all-done, bf16[2,2048,512]{2,1,0:T(8,128)(2,1)} %param.34), kind=kOutput, calls=%fused_computation.24 | convolution fusion | flops 3221225472 | bytes 13631488 | tf_op jit(solution)/shard_map/secd,edf->secf/dot_general | solution.py:168
  136.8 12.7 %convert_bitcast_fusion = bf16[4,2,192,2048]{3,2,0,1:T(8,128)(2,1)} fusion(bf16[2,512,2048]{2,1,0:T(8,128)(2,1)} %param.35, f32[2,4,192,512]{3,2,1,0:T(8,128)} %fusion.16, bf16[2,2048,512]{2,1,0:T(8,128)(2,1)} %param.33, bf16[4,2,192,2048]{3,2,1,0:T(8,128)(2,1)} %all-to-all-done), kind=kOutput, calls=%fused_computation.23 | convolution fusion | flops 6450315264 | bytes 24117248 | tf_op jit(solution)/shard_map/secf,efd->secd/dot_general | solution.py:170
  150.6 9.0 %all_gather.10 = bf16[2048,32]{0,1:T(8,128)(2,1)S(1)} all-gather(bf16[512,32]{0,1:T(8,128)(2,1)S(1)} %pad_maximum_fusion.1), channel_id=1, replica_groups=mesh['ep'=4,'tp'=8] {'ep'}, dimensions={0}, use_global_device_ids=true | all-gather | bytes 163840 | tf_op jit(solution)/shard_map/all_gather | solution.py:100
  162.3 43.4 %while.15 = (s32[]{:T(128)}, f32[512,4]{0,1:T(4,128)S(1)}, f32[512,4]{0,1:T(4,128)S(1)}, f32[512,4,64]{0,2,1:T(8,128)S(1)}, bf16[4,512,256]{2,1,0:T(8,128)(2,1)}...) while((s32[]{:T(128)}, f32[512,4]{0,1:T(4,128)S(1)}, ...), condition=%wide.region_5.6_spmd.clone, body=%wide.region_2.5_spmd.clone.sunk | while | flops 343287808 | bytes 25198720 | solution.py:119
  164.3 2.8 %fusion.90 = (f32[512,4]{0,1:T(4,128)S(1)}, f32[512,4,512]{0,2,1:T(8,128)}) fusion(bf16[512,4,32]{0,2,1:T(8,128)(2,1)S(1)} %get-tuple-element.237, bf16[4,512,32]{1,2,0:T(8,128)(2,1)S(1)} %get-tuple-element.236, s32[]{:T(128)} %get-tuple-element.219, f32[4,512,512]{2,1,0:T(8,128)S(1)} %fusion.89), kind=kOutput, calls=%fused_computation.102.clone.1 | convolution fusion | flops 70252544 | bytes 8560644 | tf_op jit(solution)/shard_map/while/body/eval_jaxpr/qhd,kd->qhk/dot_general | solution.py:43
  167.1 2.8 %fusion.91 = f32[512,4]{0,1:T(4,128)S(1)} fusion(f32[512,4,512]{0,2,1:T(8,128)} %get-tuple-element.204, f32[512,4]{0,1:T(4,128)S(1)} %select_maximum_fusion.2), kind=kLoop, calls=%fused_computation.8.clone.1 | loop fusion | flops 2095104 | bytes 4210688 | tf_op jit(solution)/shard_map/while/body/eval_jaxpr/reduce_sum | solution.py:50
  170.0 3.1 %fusion.93 = f32[512,4,64]{0,2,1:T(8,128)S(1)} fusion(bf16[512,4,64]{0,2,1:T(8,128)(2,1)S(1)} %bitcast.119, f32[512,4,512]{0,2,1:T(8,128)} %get-tuple-element.204, f32[512,4]{0,1:T(4,128)S(1)} %select_maximum_fusion.2, f32[512,4,64]{0,2,1:T(8,128)S(1)} %get-tuple-element.222, f32[512,4]{0,1:T(4,128)S(1)} %get-tuple-element.207, pred[]{:T(512)S(6)} %compare.5), kind=kOutput, calls=%fused_computation.12.clone.1 | convolution fusion | flops 136708096 | bytes 5521409 | tf_op jit(solution)/shard_map/while/body/eval_jaxpr/qhk,khd->qhd/dot_general | solution.py:51
  175.1 2.8 %fusion.90 = (f32[512,4]{0,1:T(4,128)S(1)}, f32[512,4,512]{0,2,1:T(8,128)}) fusion(bf16[512,4,32]{0,2,1:T(8,128)(2,1)S(1)} %get-tuple-element.237, bf16[4,512,32]{1,2,0:T(8,128)(2,1)S(1)} %get-tuple-element.236, s32[]{:T(128)} %get-tuple-element.219, f32[4,512,512]{2,1,0:T(8,128)S(1)} %fusion.89), kind=kOutput, calls=%fused_computation.102.clone.1 | convolution fusion | flops 70252544 | bytes 8560644 | tf_op jit(solution)/shard_map/while/body/eval_jaxpr/qhd,kd->qhk/dot_general | solution.py:43
  177.9 2.8 %fusion.91 = f32[512,4]{0,1:T(4,128)S(1)} fusion(f32[512,4,512]{0,2,1:T(8,128)} %get-tuple-element.204, f32[512,4]{0,1:T(4,128)S(1)} %select_maximum_fusion.2), kind=kLoop, calls=%fused_computation.8.clone.1 | loop fusion | flops 2095104 | bytes 4210688 | tf_op jit(solution)/shard_map/while/body/eval_jaxpr/reduce_sum | solution.py:50
  180.9 3.1 %fusion.93 = f32[512,4,64]{0,2,1:T(8,128)S(1)} fusion(bf16[512,4,64]{0,2,1:T(8,128)(2,1)S(1)} %bitcast.119, f32[512,4,512]{0,2,1:T(8,128)} %get-tuple-element.204, f32[512,4]{0,1:T(4,128)S(1)} %select_maximum_fusion.2, f32[512,4,64]{0,2,1:T(8,128)S(1)} %get-tuple-element.222, f32[512,4]{0,1:T(4,128)S(1)} %get-tuple-element.207, pred[]{:T(512)S(6)} %compare.5), kind=kOutput, calls=%fused_computation.12.clone.1 | convolution fusion | flops 136708096 | bytes 5521409 | tf_op jit(solution)/shard_map/while/body/eval_jaxpr/qhk,khd->qhd/dot_general | solution.py:51
  186.0 2.8 %fusion.90 = (f32[512,4]{0,1:T(4,128)S(1)}, f32[512,4,512]{0,2,1:T(8,128)}) fusion(bf16[512,4,32]{0,2,1:T(8,128)(2,1)S(1)} %get-tuple-element.237, bf16[4,512,32]{1,2,0:T(8,128)(2,1)S(1)} %get-tuple-element.236, s32[]{:T(128)} %get-tuple-element.219, f32[4,512,512]{2,1,0:T(8,128)S(1)} %fusion.89), kind=kOutput, calls=%fused_computation.102.clone.1 | convolution fusion | flops 70252544 | bytes 8560644 | tf_op jit(solution)/shard_map/while/body/eval_jaxpr/qhd,kd->qhk/dot_general | solution.py:43
  188.8 2.8 %fusion.91 = f32[512,4]{0,1:T(4,128)S(1)} fusion(f32[512,4,512]{0,2,1:T(8,128)} %get-tuple-element.204, f32[512,4]{0,1:T(4,128)S(1)} %select_maximum_fusion.2), kind=kLoop, calls=%fused_computation.8.clone.1 | loop fusion | flops 2095104 | bytes 4210688 | tf_op jit(solution)/shard_map/while/body/eval_jaxpr/reduce_sum | solution.py:50
  191.7 3.1 %fusion.93 = f32[512,4,64]{0,2,1:T(8,128)S(1)} fusion(bf16[512,4,64]{0,2,1:T(8,128)(2,1)S(1)} %bitcast.119, f32[512,4,512]{0,2,1:T(8,128)} %get-tuple-element.204, f32[512,4]{0,1:T(4,128)S(1)} %select_maximum_fusion.2, f32[512,4,64]{0,2,1:T(8,128)S(1)} %get-tuple-element.222, f32[512,4]{0,1:T(4,128)S(1)} %get-tuple-element.207, pred[]{:T(512)S(6)} %compare.5), kind=kOutput, calls=%fused_computation.12.clone.1 | convolution fusion | flops 136708096 | bytes 5521409 | tf_op jit(solution)/shard_map/while/body/eval_jaxpr/qhk,khd->qhd/dot_general | solution.py:51
  196.8 2.8 %fusion.90 = (f32[512,4]{0,1:T(4,128)S(1)}, f32[512,4,512]{0,2,1:T(8,128)}) fusion(bf16[512,4,32]{0,2,1:T(8,128)(2,1)S(1)} %get-tuple-element.237, bf16[4,512,32]{1,2,0:T(8,128)(2,1)S(1)} %get-tuple-element.236, s32[]{:T(128)} %get-tuple-element.219, f32[4,512,512]{2,1,0:T(8,128)S(1)} %fusion.89), kind=kOutput, calls=%fused_computation.102.clone.1 | convolution fusion | flops 70252544 | bytes 8560644 | tf_op jit(solution)/shard_map/while/body/eval_jaxpr/qhd,kd->qhk/dot_general | solution.py:43
  199.6 2.8 %fusion.91 = f32[512,4]{0,1:T(4,128)S(1)} fusion(f32[512,4,512]{0,2,1:T(8,128)} %get-tuple-element.204, f32[512,4]{0,1:T(4,128)S(1)} %select_maximum_fusion.2), kind=kLoop, calls=%fused_computation.8.clone.1 | loop fusion | flops 2095104 | bytes 4210688 | tf_op jit(solution)/shard_map/while/body/eval_jaxpr/reduce_sum | solution.py:50
  202.6 3.1 %fusion.93 = f32[512,4,64]{0,2,1:T(8,128)S(1)} fusion(bf16[512,4,64]{0,2,1:T(8,128)(2,1)S(1)} %bitcast.119, f32[512,4,512]{0,2,1:T(8,128)} %get-tuple-element.204, f32[512,4]{0,1:T(4,128)S(1)} %select_maximum_fusion.2, f32[512,4,64]{0,2,1:T(8,128)S(1)} %get-tuple-element.222, f32[512,4]{0,1:T(4,128)S(1)} %get-tuple-element.207, pred[]{:T(512)S(6)} %compare.5), kind=kOutput, calls=%fused_computation.12.clone.1 | convolution fusion | flops 136708096 | bytes 5521409 | tf_op jit(solution)/shard_map/while/body/eval_jaxpr/qhk,khd->qhd/dot_general | solution.py:51
  205.8 2.1 convolution_convert_fusion
  207.9 11.8 %reduce-scatter.5.cloned.1.call-done = bf16[4,2,192,256]{3,2,0,1:T(8,128)(2,1)} async-done(((bf16[4,2,192,2048]{3,2,0,1:T(8,128)(2,1)}), bf16[4,2,192,256]{3,2,0,1:T(8,128)(2,1)}) %reduce-scatter.5.cloned.1.call-update) | async-done | bytes 786448 | tf_op jit(solution)/shard_map/reduce_scatter | solution.py:173
  219.7 2.1 copy.43
  221.9 3.7 %all-to-all-start.1 = ((bf16[4,2,192,256]{3,2,1,0:T(8,128)(2,1)}), bf16[4,2,192,256]{3,2,1,0:T(8,128)(2,1)S(1)}, u32[]{:S(2)}, u32[]{:S(2)}) async-start(bf16[4,2,192,256]{3,2,1,0:T(8,128)(2,1)} %copy.43), calls=%async_computation.3 | async-start | bytes 1572864 | tf_op jit(solution)/shard_map/all_to_all | solution.py:176
  225.8 9.0 %all-to-all-done.1 = bf16[4,2,192,256]{3,2,1,0:T(8,128)(2,1)S(1)} async-done(((bf16[4,2,192,256]{3,2,1,0:T(8,128)(2,1)}), bf16[4,2,192,256]{3,2,1,0:T(8,128)(2,1)S(1)}, u32[]{:S(2)}, u32[]{:S(2)}) %all-to-all-start.1) | async-done | bytes 786464 | tf_op jit(solution)/shard_map/all_to_all | solution.py:176
  234.7 3.9 %gather_fusion.1 = bf16[1024,256]{1,0:T(8,128)(2,1)S(1)} fusion(bf16[1536,256]{1,0:T(8,128)(2,1)S(1)} %bitcast.118, s32[1024]{0:T(1024)S(1)} %broadcast_clamp_fusion), kind=kCustom, calls=%fused_computation.1 | custom fusion | bytes 1052672 | tf_op jit(solution)/shard_map/gather | solution.py:177
  239.2 3.6 %multiply_reduce_fusion = bf16[512,256]{1,0:T(8,128)(2,1)} fusion(f32[512,2,256]{2,1,0:T(2,128)S(1)} %reshape.190, f32[512,2]{1,0:T(8,128)S(1)} %copy.44), kind=kLoop, calls=%fused_computation.59 | loop fusion | flops 393216 | bytes 1314816 | tf_op jit(solution)/shard_map/reduce_sum | solution.py:179
  242.8 14.3 %reduce-scatter.3.cloned.1.call-done = bf16[64,2048]{1,0:T(8,128)(2,1)} async-done(((bf16[512,2048]{1,0:T(8,128)(2,1)}), bf16[64,2048]{1,0:T(8,128)(2,1)}) %reduce-scatter.3.cloned.1.call-update) | async-done | bytes 262160 | tf_op jit(solution)/shard_map/reduce_scatter | solution.py:134
  (102 shorter events, 20.6 us)
Async XLA Ops:
  8.0 197.8 %copy-start = (bf16[256,2048]{1,0:T(8,128)(2,1)S(1)}, bf16[256,2048]{1,0:T(8,128)(2,1)}, u32[]{:S(2)}) copy-start(bf16[256,2048]{1,0:T(8,128)(2,1)} %param.28) | copy-start | bytes 3145732
  42.5 5.4 %copy-start.3 = (bf16[512,512]{1,0:T(8,128)(2,1)S(1)}, bf16[512,512]{1,0:T(8,128)(2,1)}, u32[]{:S(2)}) copy-start(bf16[512,512]{1,0:T(8,128)(2,1)} %param.20) | copy-start | bytes 1572868
  42.5 5.6 %copy-start.6 = (bf16[512,256]{1,0:T(8,128)(2,1)S(1)}, bf16[512,256]{1,0:T(8,128)(2,1)}, u32[]{:S(2)}) copy-start(bf16[512,256]{1,0:T(8,128)(2,1)} %param.26) | copy-start | bytes 786436
  42.5 5.6 %copy-start.10 = (f32[512]{0:T(512)S(1)}, f32[512]{0:T(512)}, u32[]{:S(2)}) copy-start(f32[512]{0:T(512)} %param.23) | copy-start | bytes 6148
  42.5 6.8 %copy-start.7 = (bf16[512,256]{1,0:T(8,128)(2,1)S(1)}, bf16[512,256]{1,0:T(8,128)(2,1)}, u32[]{:S(2)}) copy-start(bf16[512,256]{1,0:T(8,128)(2,1)} %param.27) | copy-start | bytes 786436
  42.5 85.3 %all-to-all-start = ((bf16[4,2,192,2048]{3,2,1,0:T(8,128)(2,1)}), bf16[4,2,192,2048]{3,2,1,0:T(8,128)(2,1)}, u32[]{:S(2)}, u32[]{:S(2)}) async-start(bf16[4,2,192,2048]{3,2,1,0:T(8,128)(2,1)} %broadcast_multiply_fusion), calls=%async_computation.1 | async-start | bytes 12582912 | tf_op jit(solution)/shard_map/all_to_all | solution.py:164
  47.8 114.4 %all-gather.3.cloned.1.call-start = ((), (), s32[]{:S(2)}) async-start(), calls=%async_computation.4 | async-start | bytes 1310720 | tf_op jit(solution)/shard_map/all_gather | solution.py:98
  49.2 113.1 %all-gather.5.cloned.1.call-start = ((), (), s32[]{:S(2)}) async-start(), calls=%async_computation.5 | async-start | bytes 1310720 | tf_op jit(solution)/shard_map/all_gather | solution.py:99
  50.4 169.4 %reduce-scatter.5.cloned.1.call-start = ((), (), s32[]{:S(2)}) async-start(), calls=%async_computation.7 | async-start | bytes 7077888 | tf_op jit(solution)/shard_map/reduce_scatter | solution.py:173
  149.5 0.8 copy-start.4
  149.5 10.1 %copy-start.1 = (bf16[512,1024]{1,0:T(8,128)(2,1)S(1)}, bf16[512,1024]{1,0:T(8,128)(2,1)}, u32[]{:S(2)}) copy-start(bf16[512,1024]{1,0:T(8,128)(2,1)} %param.19) | copy-start | bytes 3145732
  149.5 10.4 %copy-start.8 = (bf16[1024,128]{1,0:T(8,128)(2,1)S(1)}, bf16[1024,128]{1,0:T(8,128)(2,1)}, u32[]{:S(2)}) copy-start(bf16[1024,128]{1,0:T(8,128)(2,1)} %param.25) | copy-start | bytes 786436
  149.5 10.4 %copy-start.9 = (f32[1024]{0:T(1024)S(1)}, f32[1024]{0:T(1024)}, u32[]{:S(2)}) copy-start(f32[1024]{0:T(1024)} %param.22) | copy-start | bytes 12292
  149.6 107.5 %reduce-scatter.3.cloned.1.call-start = ((), (), s32[]{:S(2)}) async-start(), calls=%async_computation.6 | async-start | bytes 2359296 | tf_op jit(solution)/shard_map/reduce_scatter | solution.py:134
  150.3 10.3 %copy-start.2 = (bf16[512,1024]{1,0:T(8,128)(2,1)S(1)}, bf16[512,1024]{1,0:T(8,128)(2,1)}, u32[]{:S(2)}) copy-start(bf16[512,1024]{1,0:T(8,128)(2,1)} %param.19) | copy-start | bytes 3145732
  205.8 19.8 %copy-start.5 = (f32[512,2]{0,1:T(2,128)S(1)}, f32[512,2]{0,1:T(2,128)}, u32[]{:S(2)}) copy-start(f32[512,2]{0,1:T(2,128)} %param.32) | copy-start | bytes 12292
  221.9 12.9 %all-to-all-start.1 = ((bf16[4,2,192,256]{3,2,1,0:T(8,128)(2,1)}), bf16[4,2,192,256]{3,2,1,0:T(8,128)(2,1)S(1)}, u32[]{:S(2)}, u32[]{:S(2)}) async-start(bf16[4,2,192,256]{3,2,1,0:T(8,128)(2,1)} %copy.43), calls=%async_computation.3 | async-start | bytes 1572864 | tf_op jit(solution)/shard_map/all_to_all | solution.py:176
Sparse Core Ops, SparseCore 0:
  51.1 59.6 all-gather.2
  113.2 44.5 all-gather.4
Sparse Core Ops, SparseCore 1:
  149.7 70.0 reduce-scatter.4
  222.5 34.6 reduce-scatter.2
where the time goes:
time: 265 us
  waiting for transfers between devices  112 us (42%)
  matrix products  54.7 us (21%)
  local copies, waits for them, and re-layouts  33.8 us (13%)
  other arithmetic  29.1 us (11%)
  between operations  15.9 us (6%)
  starting transfers between devices  9.44 us (4%)
  blocking collectives  9.03 us (3%)
    all_to_all x1, waiting for transfers between devices, experts(): lax.all_to_all(outgoing, 'ep', split_axis=0, concat_axis=0, tiled=True)  77.1 us
    reduce_scatter x1, waiting for transfers between devices, token_mixer(): lax.psum_scatter(jnp.dot(attended, output_weight, preferred_element_type=...  14.3 us
    dot_general x1, matrix products, experts(): jnp.einsum('secf,efd->secd', hidden, down_weight, preferred_element_type=...  12.7 us
    dot_general x4, matrix products, attend_block(): jnp.einsum('qhk,khd->qhd', expo.astype(jnp.bfloat16), value_block, prefer...  12.3 us
    reduce_scatter x1, waiting for transfers between devices, experts(): lax.psum_scatter(partial_value.astype(jnp.bfloat16), 'tp', scatter_dimens...  11.8 us
    reduce_sum x4, other arithmetic, attend_block(): row_total = row_total * factor + jnp.sum(expo, axis=-1)  11.2 us
    dot_general x4, matrix products, attend_block(): jnp.einsum('qhd,kd->qhk', query_turned, turned_block, preferred_element_t...  11.1 us
    dot_general x1, matrix products, experts(): jnp.einsum('secd,edf->secf', arrived, up_weight, preferred_element_type=j...  9.08 us
  transfers between devices with their start and end apart: 6, of which 4 were waited for; matrix products, arithmetic and copies ran while one was open for 31% of the time, Pallas kernels for 0%

commit v1 on v0

v1 whole, which is shorter than its diff:
```python
import functools

import jax
import jax.numpy as jnp
from jax import lax
from jax.experimental import pallas as pl
from jax.experimental.pallas import tpu as pltpu
from jax.sharding import PartitionSpec as P

NOPE = 64
VDIM = 64

NORM_EPSILON = 1e-06
ROTARY_BASE = 10000.0
F32 = jnp.float32
BF16 = jnp.bfloat16


def norm_rows(source, gain_vector):
    as_float = source.astype(F32)
    factor = lax.rsqrt(jnp.mean(as_float * as_float, axis=-1, keepdims=True) + NORM_EPSILON)
    return (as_float * factor * gain_vector).astype(BF16)


def rotation_tables(positions, width, copies):
    half_width = width // 2
    lane = jnp.arange(width * copies, dtype=jnp.int32) % width
    frequencies = ROTARY_BASE ** (-(lane % half_width).astype(F32) / half_width)
    angles = positions[:, None] * frequencies[None, :]
    sign = jnp.where(lane < half_width, -1.0, 1.0).astype(F32)
    return jnp.cos(angles), jnp.sin(angles) * sign[None, :]


def swap_matrix(width, copies):
    half_width = width // 2
    lane = jnp.arange(width * copies, dtype=jnp.int32)
    partner = (lane // width) * width + (lane % width + half_width) % width
    return (lane[:, None] == partner[None, :]).astype(BF16)


def attention_kernel(head_count, turn_width, scale, q_ref, qt_ref, kt_ref, tk_ref, v_ref, out_ref):
    turned_keys = tk_ref[...]
    pieces = []
    per_pair = 128 // VDIM
    for head in range(head_count):
        query = jnp.concatenate(
            [
                q_ref[:, head * NOPE : (head + 1) * NOPE],
                qt_ref[:, head * turn_width : (head + 1) * turn_width],
            ],
            axis=1,
        )
        keys = jnp.concatenate([kt_ref[head * NOPE : (head + 1) * NOPE, :], turned_keys], axis=0)
        scores = jnp.dot(query, keys, preferred_element_type=F32) * scale
        top = jnp.max(scores, axis=-1, keepdims=True)
        expo = jnp.exp(scores - top)
        total = jnp.sum(expo, axis=-1, keepdims=True)
        pair = head // per_pair
        mixed = jnp.dot(
            expo.astype(BF16), v_ref[:, pair * 128 : (pair + 1) * 128], preferred_element_type=F32
        )
        inner = head % per_pair
        mixed = mixed[:, inner * VDIM : (inner + 1) * VDIM]
        pieces.append((mixed / total).astype(BF16))
    out_ref[...] = jnp.concatenate(pieces, axis=1)


def attention(query_plain, query_turned, keys_t, turned_t, values, turn_width):
    rows, width = query_plain.shape
    tokens = values.shape[0]
    head_count = width // NOPE
    block = 128
    scale = (NOPE + turn_width) ** (-0.5)
    whole = lambda i: (0, 0)
    return pl.pallas_call(
        functools.partial(attention_kernel, head_count, turn_width, scale),
        grid=(rows // block,),
        in_specs=[
            pl.BlockSpec((block, width), lambda i: (i, 0)),
            pl.BlockSpec((block, query_turned.shape[1]), lambda i: (i, 0)),
            pl.BlockSpec(keys_t.shape, whole),
            pl.BlockSpec(turned_t.shape, whole),
            pl.BlockSpec(values.shape, whole),
        ],
        out_specs=pl.BlockSpec((block, head_count * VDIM), lambda i: (i, 0)),
        out_shape=jax.ShapeDtypeStruct((rows, head_count * VDIM), BF16),
        compiler_params=pltpu.CompilerParams(vmem_limit_bytes=40 * 1024 * 1024),
        cost_estimate=pl.CostEstimate(
            flops=40 * rows * tokens * head_count * (NOPE + turn_width),
            bytes_accessed=4 * tokens * width,
            transcendentals=rows * tokens * head_count,
        ),
        name="attention",
    )(query_plain, query_turned, keys_t, turned_t, values)


def half_of(source, parity, axis):
    half = source.shape[axis] // 2
    return lax.dynamic_slice_in_dim(source, parity * half, half, axis)


def swap_cores(source):
    size = lax.axis_size("tp")
    return lax.ppermute(source, "tp", [(i, i ^ 1) for i in range(size)])


def latent_part(joint_latent, rotary_key, joint_gain, parity):
    row_count = joint_latent.shape[0]
    turn_width = rotary_key.shape[1]
    positions = (lax.axis_index("ep") * row_count + jnp.arange(row_count, dtype=jnp.int32)).astype(F32)
    normed = half_of(norm_rows(joint_latent, joint_gain), parity, 1)
    cosine, sine = rotation_tables(positions, turn_width, 1)
    swapped = jnp.dot(rotary_key, swap_matrix(turn_width, 1), preferred_element_type=F32)
    turned = (rotary_key.astype(F32) * cosine + swapped * sine).astype(BF16)
    return jnp.concatenate([normed, turned], axis=1)


def token_mixer(
    latent,
    query_latent,
    query_gain,
    query_weight,
    query_rotary,
    key_weight,
    value_weight,
    turn_width,
    parity,
):
    mine, other, turned = latent
    row_count = query_latent.shape[0]
    positions = (lax.axis_index("ep") * row_count + jnp.arange(row_count, dtype=jnp.int32)).astype(F32)
    head_count = key_weight.shape[1] // NOPE
    query_normed = norm_rows(query_latent, query_gain)
    query_plain = jnp.dot(query_normed, query_weight, preferred_element_type=F32).astype(BF16)
    cosine, sine = rotation_tables(positions, turn_width, head_count)
    rotary_swapped = jnp.dot(
        query_rotary, swap_matrix(turn_width, head_count), preferred_element_type=F32
    ).astype(BF16)
    query_turned = (
        jnp.dot(query_normed, query_rotary, preferred_element_type=F32) * cosine
        + jnp.dot(query_normed, rotary_swapped, preferred_element_type=F32) * sine
    ).astype(BF16)

    normed = jnp.where(
        parity == 0,
        jnp.concatenate([mine, other], axis=1),
        jnp.concatenate([other, mine], axis=1),
    )
    keys_t = jnp.einsum("td,df->ft", normed, key_weight, preferred_element_type=F32).astype(BF16)
    values = jnp.dot(normed, value_weight, preferred_element_type=F32).astype(BF16)
    return attention(query_plain, query_turned, keys_t, turned.T, values, turn_width)


def column_blocks(weight, parity, blocks):
    width = weight.shape[2] // blocks
    return jnp.concatenate(
        [
            lax.dynamic_slice_in_dim(weight, (2 * z + parity) * width, width, 2)
            for z in range(blocks // 2)
        ],
        axis=2,
    )


def local(
    query_latent,
    joint_latent,
    rotary_key,
    query_gain,
    joint_gain,
    query_weight,
    query_rotary,
    key_weight,
    value_weight,
    output_weight,
    expert_input,
    expert_gain,
    routes,
    route_weight,
    gate_weight,
    up_weight,
    down_weight,
):
    parity = lax.axis_index("tp") % 2
    tp_size = lax.axis_size("tp")
    row_count, feature_width = expert_input.shape
    group_count = lax.axis_size("ep")
    local_count = gate_weight.shape[0]
    expert_count = local_count * group_count
    capacity = 3 * row_count // (2 * group_count)
    half = feature_width // 2

    part = latent_part(joint_latent, rotary_key, joint_gain, parity)
    part, expert_rows = lax.optimization_barrier((part, expert_input))
    gathered = lax.all_gather(part, "ep", axis=0, tiled=True)

    routes_t = routes.T
    names = jnp.arange(expert_count, dtype=jnp.int32)
    member = (routes_t[0][None, :] == names[:, None]) | (routes_t[1][None, :] == names[:, None])
    token = jnp.arange(row_count, dtype=jnp.int32)
    before = (token[:, None] < token[None, :]).astype(BF16)
    rank = jnp.dot(member.astype(BF16), before, preferred_element_type=F32).astype(jnp.int32)
    place = jnp.where(member, rank, -1)
    slots = jnp.arange(capacity, dtype=jnp.int32)
    chosen = (place[:, None, :] == slots[None, :, None]).astype(BF16)
    chosen = chosen.reshape(expert_count * capacity, row_count)
    rows_half = lax.optimization_barrier(half_of(norm_rows(expert_rows, expert_gain), parity, 1))
    outgoing = jnp.dot(chosen, rows_half, preferred_element_type=F32).astype(BF16)
    outgoing = outgoing.reshape(group_count, local_count, capacity, half)
    mine = lax.all_to_all(outgoing, "ep", split_axis=0, concat_axis=0, tiled=True)
    latent_half = gathered[:, : joint_latent.shape[1] // 2]
    attended = token_mixer(
        (latent_half, swap_cores(latent_half), gathered[:, joint_latent.shape[1] // 2 :]),
        query_latent,
        query_gain,
        query_weight,
        query_rotary,
        key_weight,
        value_weight,
        rotary_key.shape[1],
        parity,
    )
    mine, attended = lax.optimization_barrier((mine, attended))
    other = swap_cores(mine)
    mixer_out = lax.psum_scatter(
        jnp.dot(attended, output_weight, preferred_element_type=F32).astype(BF16),
        "tp",
        scatter_dimension=0,
        tiled=True,
    )

    def project(weight):
        return jnp.einsum(
            "secd,edf->secf", mine, half_of(weight, parity, 1), preferred_element_type=F32
        ) + jnp.einsum(
            "secd,edf->secf", other, half_of(weight, 1 - parity, 1), preferred_element_type=F32
        )

    gate_acts = project(gate_weight)
    up_acts = project(up_weight)
    hidden = (jax.nn.silu(gate_acts) * up_acts).astype(BF16)

    def down(side):
        return jnp.einsum(
            "secf,efd->secd",
            hidden,
            column_blocks(down_weight, side, tp_size),
            preferred_element_type=F32,
        ).astype(BF16)

    theirs = swap_cores(down(1 - parity))
    summed = (down(parity).astype(F32) + theirs.astype(F32)).astype(BF16)
    returned = lax.all_to_all(summed, "ep", split_axis=0, concat_axis=0, tiled=True)
    returned = returned.reshape(expert_count * capacity, half)

    def picked(k):
        slot = jnp.sum(
            jnp.where(routes_t[k][None, :] == names[:, None], names[:, None] * capacity + rank, 0),
            axis=0,
        )
        every = jnp.arange(expert_count * capacity, dtype=jnp.int32)
        pick = (slot[:, None] == every[None, :]).astype(BF16)
        return jnp.dot(pick, returned, preferred_element_type=F32) * route_weight[:, k : k + 1]

    combined = (picked(0) + picked(1)).astype(BF16)
    groups = [list(range(side, tp_size, 2)) for side in range(2)]
    expert_out = lax.psum_scatter(
        combined, "tp", scatter_dimension=1, axis_index_groups=groups, tiled=True
    )
    return (mixer_out, expert_out)


def solution(mesh):
    return jax.shard_map(
        local,
        mesh=mesh,
        in_specs=(
            P("ep", None),
            P("ep", None),
            P("ep", None),
            P(),
            P(),
            P(None, "tp"),
            P(None, "tp"),
            P(None, "tp"),
            P(None, "tp"),
            P("tp", None),
            P("ep", None),
            P(),
            P("ep", None),
            P("ep", None),
            P("ep", None, "tp"),
            P("ep", None, "tp"),
            P("ep", "tp", None),
        ),
        out_specs=(P(("ep", "tp"), None), P("ep", "tp")),
        check_vma=False,
    )
```

time: 265 us -> 210 us (0.79)
  local copies, waits for them, and re-layouts: 33.8 us -> 14 us
  other arithmetic: 29.1 us -> 10.9 us
  waiting for transfers between devices: 112 us -> 100 us
  Pallas kernels: 0 us -> 9.74 us
  blocking collectives: 9.03 us -> 0 us
  matrix products: 54.7 us -> 49.3 us
    all_to_all x2, waiting for transfers between devices: 86.1 us -> 36.7 us  [the longest x1 36.7 us: local(): lax.all_to_all(summed, 'ep', split_axis=0, concat_axis=0, tiled=True)]
    all_gather x2 -> x1, waiting for transfers between devices: 0.04 us -> 31.8 us  [local(): gathered = lax.all_gather(part, 'ep', axis=0, tiled=True)]
    reduce_sum x6 -> x0, other arithmetic: 14.8 us -> none  [the longest x4 11.2 us: attend_block(): row_total = row_total * factor + jnp.sum(expo, axis=-1)]
    scatter x2 -> x0, local copies, waits for them, and re-layouts: 11.9 us -> none  [the longest x1 7.59 us: experts(): jnp.zeros((expert_count * capacity,), jnp.bfloat16).at[slot_index].set(1.0)]
    gather x2 -> x0, local copies, waits for them, and re-layouts: 11 us -> none  [the longest x1 7.1 us: experts(): normed[slot_token] * filled[:, None]]
    pallas_call x0 -> x1, Pallas kernels: none -> 9.74 us  [attention(): pl.pallas_call(functools.partial(attention_kernel, head_count, turn_width...]
    all_gather x1 -> x0, blocking collectives: 9.03 us -> none  [token_mixer(): turned_piece = lax.all_gather(turned_key, 'ep', axis=0, tiled=True)]
    mul x2 -> x1, other arithmetic: 6.61 us -> 0.01 us  [picked(): names[:, None] * capacity + rank]
  transfers between devices with their start and end apart: 6 -> 8, of which waited for: 4 -> 4; matrix products, arithmetic and copies ran while one was open for 31% -> 24% of each run, Pallas kernels for 0% -> 5%
where the time goes in v1:
time: 210 us; the launch traced here: 209 us
  waiting for transfers between devices  100 us (48%)
  matrix products  49.3 us (23%)
  between operations  14.2 us (7%)
  local copies, waits for them, and re-layouts  14 us (7%)
  other arithmetic  10.9 us (5%)
  starting transfers between devices  10.8 us (5%)
  Pallas kernels  9.74 us (5%)
    all_to_all x1, waiting for transfers between devices, local(): lax.all_to_all(summed, 'ep', split_axis=0, concat_axis=0, tiled=True)  36.7 us
    all_gather x1, waiting for transfers between devices, local(): gathered = lax.all_gather(part, 'ep', axis=0, tiled=True)  31.8 us
    reduce_scatter x1, waiting for transfers between devices, local(): lax.psum_scatter(combined, 'tp', scatter_dimension=1, axis_index_groups=g...  27.9 us
    pallas_call x1, Pallas kernels, attention(): pl.pallas_call(functools.partial(attention_kernel, head_count, turn_width...  9.74 us
    dot_general x2, matrix products, picked(): jnp.dot(pick, returned, preferred_element_type=F32)  8.54 us
    dot_general x2, matrix products, project(): jnp.einsum('secd,edf->secf', other, half_of(weight, 1 - parity, 1), prefe...  7.95 us
    dot_general x2, matrix products, down(): jnp.einsum('secf,efd->secd', hidden, column_blocks(down_weight, side, tp_...  7.76 us
    dot_general x2, matrix products, project(): jnp.einsum('secd,edf->secf', mine, half_of(weight, parity, 1), preferred_...  7.51 us
  transfers between devices with their start and end apart: 8, of which 4 were waited for; matrix products, arithmetic and copies ran while one was open for 24% of the time, Pallas kernels for 5%

profile of v1, /device:TPU:0, one launch (start us, length us, event | category | flops | bytes accessed | tf_op | source)
XLA Modules:
  0.0 209.3 jit_solution(14046167022091732898)
XLA Ops:
  7.3 2.2 %copy.26 = bf16[512,512]{0,1:T(8,128)(2,1)} copy(bf16[512,512]{1,0:T(8,128)(2,1)} %param.18) | data formatting | bytes 1048576 | tf_op args[1]
  9.5 2.2 %convert_element_type.109 = f32[512,512]{0,1:T(8,128)} convert(bf16[512,512]{0,1:T(8,128)(2,1)} %copy.26) | non-fusion elementwise | flops 262144 | bytes 1572864 | tf_op jit(solution)/shard_map/convert_element_type | solution.py:20
  11.7 1.2 multiply_reduce_fusion.1
  13.0 1.1 fusion.49
  15.3 2.5 %convert_element_type.115 = f32[512,2048]{1,0:T(8,128)} convert(bf16[512,2048]{1,0:T(8,128)(2,1)S(1)} %copy-done.1) | non-fusion elementwise | flops 1048576 | bytes 6291456 | tf_op jit(solution)/shard_map/convert_element_type | solution.py:20
  18.3 1.8 fusion.12
  21.6 3.5 %convolution_convert_fusion = bf16[1536,1024]{1,0:T(8,128)(2,1)} fusion(pred[1536,512]{1,0:T(32,128)(4,1)S(1)} %bitcast_compare_fusion, bf16[512,1024]{1,0:T(8,128)(2,1)S(1)} %fusion.12), kind=kOutput, calls=%fused_computation.3 | convolution fusion | flops 1612185600 | bytes 4980736 | tf_op jit(solution)/shard_map/dot_general | solution.py:208
  25.0 5.3 %all-to-all-start = ((bf16[4,2,192,1024]{3,2,1,0:T(8,128)(2,1)}), bf16[4,2,192,1024]{3,2,1,0:T(8,128)(2,1)}, u32[]{:S(2)}, u32[]{:S(2)}) async-start(bf16[4,2,192,1024]{3,2,1,0:T(8,128)(2,1)} %bitcast.92), calls=%async_computation | async-start | bytes 6291456 | tf_op jit(solution)/shard_map/all_to_all | solution.py:210
  30.7 1.9 convolution_multiply_fusion
  32.6 31.8 %all-gather.2.cloned.1.call-done = bf16[2048,288]{0,1:T(8,128)(2,1)} async-done(((bf16[512,288]{0,1:T(8,128)(2,1)}), bf16[2048,288]{0,1:T(8,128)(2,1)}) %all-gather.2.cloned.1.call-update) | async-done | bytes 1179664 | tf_op jit(solution)/shard_map/all_gather | solution.py:195
  64.4 1.3 slice.28
  65.8 2.4 %fusion.44.qt_ref = bf16[512,128]{1,0:T(8,128)(2,1)S(1)} fusion(f32[512,128]{1,0:T(8,128)} %convolution_multiply_fusion, bf16[1024,128]{1,0:T(8,128)(2,1)} %param.23, f32[128]{0:T(128)S(1)} %get-tuple-element.25, f32[128]{0:T(128)S(1)} %get-tuple-element.26, f32[512]{0:T(512)S(1)} %add_convert_fusion.1, s32[128]{0:T(128)S(1)} %fusion.69, ...), kind=kOutput, calls=%fused_computation.65 | convolution fusion | flops 170360832 | bytes 1713664 | tf_op jit(solution)/shard_map/dot_general | solution.py:141
  68.2 1.5 convolution_convert_fusion.5.q_ref
  70.7 2.5 %fusion.7.kt_ref = bf16[256,2048]{1,0:T(8,128)(2,1)S(1)} fusion(bf16[512,256]{1,0:T(8,128)(2,1)} %param.24, bf16[2048,256]{0,1:T(8,128)(2,1)} %collective-permute-done, bf16[2048,256]{0,1:T(8,128)(2,1)S(1)} %slice.28, pred[]{:T(512)S(6)} %eq.151), kind=kOutput, calls=%fused_computation.22 | convolution fusion | flops 546832384 | bytes 3407873 | tf_op jit(solution)/shard_map/td,df->ft/dot_general | solution.py:149
  73.3 2.5 %convolution_convert_fusion.2.v_ref = bf16[2048,256]{1,0:T(8,128)(2,1)S(1)} fusion(bf16[512,256]{1,0:T(8,128)(2,1)S(1)} %copy-done.10, bf16[2048,256]{0,1:T(8,128)(2,1)} %collective-permute-done, bf16[2048,256]{0,1:T(8,128)(2,1)S(1)} %slice.28, pred[]{:T(512)S(6)} %eq.151), kind=kOutput, calls=%fused_computation.20 | convolution fusion | flops 546832384 | bytes 3407873 | tf_op jit(solution)/shard_map/dot_general | solution.py:150
  75.7 9.7 %attention.1 = bf16[512,256]{1,0:T(8,128)(2,1)S(1)} custom-call(bf16[512,256]{1,0:T(8,128)(2,1)S(1)} %convolution_convert_fusion.5.q_ref, bf16[512,128]{1,0:T(8,128)(2,1)S(1)} %fusion.44.qt_ref, bf16[256,2048]{1,0:T(8,128)(2,1)S(1)} %fusion.7.kt_ref, bf16[32,2048]{1,0:T(8,128)(2,1)S(1)} %slice_bitcast_fusion.tk_ref, ...), custom_call_target="tpu_custom_call" | custom-call | flops 16106127360 | bytes 2097152 | tf_op jit(solution)/shard_map/attention/pallas_call | solution.py:75
  85.5 3.9 %copy.28 = bf16[4,2,192,1024]{3,2,0,1:T(8,128)(2,1)} copy(bf16[4,2,192,1024]{3,2,1,0:T(8,128)(2,1)} %all-to-all-done) | data formatting | bytes 6291456 | tf_op jit(solution)/shard_map/optimization_barrier | solution.py:223
  89.9 2.7 %constant_dynamic-slice_fusion.7 = (bf16[2,512,256]{2,1,0:T(8,128)(2,1)S(1)}, bf16[2,512,256]{2,1,0:T(8,128)(2,1)S(1)}, bf16[2,512,256]{2,1,0:T(8,128)(2,1)S(1)}...) fusion(bf16[2,512,2048]{2,1,0:T(8,128)(2,1)} %param.33, ...), kind=kLoop, calls=%fused_computation.109 | loop fusion | bytes 8388640 | tf_op jit(solution)/shard_map/dynamic_slice | solution.py:158
  93.4 3.8 %fusion.27 = f32[2,512,4,192]{1,3,2,0:T(8,128)S(1)} fusion(bf16[2,2048,512]{2,1,0:T(8,128)(2,1)S(1)} %copy-done.8, s32[]{:T(128)S(6)} %select_n.179, bf16[4,2,192,1024]{3,2,1,0:T(8,128)(2,1)} %all-to-all-done), kind=kOutput, calls=%fused_computation.46 | convolution fusion | flops 1610612736 | bytes 8388612 | tf_op jit(solution)/shard_map/secd,edf->secf/dot_general | solution.py:233
  97.2 3.7 %fusion.31 = f32[2,512,4,192]{1,3,2,0:T(8,128)S(1)} fusion(bf16[2,2048,512]{2,1,0:T(8,128)(2,1)S(1)} %copy-done.7, s32[]{:T(128)S(6)} %select_n.179, bf16[4,2,192,1024]{3,2,1,0:T(8,128)(2,1)} %all-to-all-done), kind=kOutput, calls=%fused_computation.50 | convolution fusion | flops 1610612736 | bytes 8388612 | tf_op jit(solution)/shard_map/secd,edf->secf/dot_general | solution.py:233
  100.9 3.7 %fusion.29 = f32[2,512,4,192]{1,3,2,0:T(8,128)S(1)} fusion(bf16[4,2,192,1024]{3,2,0,1:T(8,128)(2,1)} %collective-permute-done.1, bf16[2,2048,512]{2,1,0:T(8,128)(2,1)S(1)} %copy-done.7, s32[]{:T(128)S(6)} %select_n.192), kind=kOutput, calls=%fused_computation.48 | convolution fusion | flops 1610612736 | bytes 8388612 | tf_op jit(solution)/shard_map/secd,edf->secf/dot_general | solution.py:235
  104.6 4.3 %fusion.1 = bf16[4,2,192,512]{3,2,0,1:T(8,128)(2,1)S(1)} fusion(f32[2,512,4,192]{1,3,2,0:T(8,128)S(1)} %fusion.27, f32[2,512,4,192]{1,3,2,0:T(8,128)S(1)} %fusion.31, f32[2,512,4,192]{1,3,2,0:T(8,128)S(1)} %fusion.29, bf16[4,2,192,1024]{3,2,0,1:T(8,128)(2,1)} %collective-permute-done.1, bf16[2,2048,512]{2,1,0:T(8,128)(2,1)S(1)} %copy-done.8, s32[]{:T(128)S(6)} %select_n.192), kind=kOutput, calls=%fused_computation.5 | convolution fusion | flops 1616904192 | bytes 16252932 | tf_op jit(solution)/shard_map/secd,edf->secf/dot_general | solution.py:235
  108.9 3.2 %convert_bitcast_fusion = bf16[4,2,192,1024]{3,2,0,1:T(8,128)(2,1)} fusion(bf16[4,2,192,512]{3,2,0,1:T(8,128)(2,1)S(1)} %fusion.1, bf16[2,512,256]{2,1,0:T(8,128)(2,1)S(1)} %get-tuple-element.18, bf16[2,512,256]{2,1,0:T(8,128)(2,1)S(1)} %get-tuple-element.19, bf16[2,512,256]{2,1,0:T(8,128)(2,1)S(1)} %get-tuple-element.13, ...), kind=kOutput, calls=%fused_computation.13 | convolution fusion | flops 1620574208 | bytes 6815744 | tf_op jit(solution)/shard_map/secf,efd->secd/dot_general | solution.py:244
  112.1 2.1 convolution_convert_fusion.1
  114.2 3.9 %collective-permute-done.2 = bf16[4,2,192,1024]{3,2,0,1:T(8,128)(2,1)} collective-permute-done((bf16[4,2,192,1024]{3,2,0,1:T(8,128)(2,1)}, bf16[4,2,192,1024]{3,2,0,1:T(8,128)(2,1)}, u32[]{:S(2)}, u32[]{:S(2)}) %collective-permute-start.2) | collective-permute-done | bytes 3145760 | tf_op jit(solution)/shard_map/ppermute | solution.py:104
  118.1 4.6 %fusion = bf16[4,2,192,1024]{3,2,0,1:T(8,128)(2,1)S(1)} fusion(bf16[4,2,192,1024]{3,2,0,1:T(8,128)(2,1)} %collective-permute-done.2, bf16[4,2,192,512]{3,2,0,1:T(8,128)(2,1)} %copy-done.13, bf16[2,512,256]{2,1,0:T(8,128)(2,1)S(1)} %get-tuple-element.15, bf16[2,512,256]{2,1,0:T(8,128)(2,1)S(1)} %get-tuple-element.16, ...), kind=kOutput, calls=%fused_computation.1 | convolution fusion | flops 1626865664 | bytes 9961472 | tf_op jit(solution)/shard_map/secf,efd->secd/dot_general | solution.py:244
  122.7 2.0 copy.31
  124.7 4.8 %all-to-all-start.1 = ((bf16[4,2,192,1024]{3,2,1,0:T(8,128)(2,1)}), bf16[4,2,192,1024]{3,2,1,0:T(8,128)(2,1)}, u32[]{:S(2)}, u32[]{:S(2)}) async-start(bf16[4,2,192,1024]{3,2,1,0:T(8,128)(2,1)} %copy.31), calls=%async_computation.2 | async-start | bytes 6291456 | tf_op jit(solution)/shard_map/all_to_all | solution.py:253
  129.5 36.7 %all-to-all-done.1 = bf16[4,2,192,1024]{3,2,1,0:T(8,128)(2,1)} async-done(((bf16[4,2,192,1024]{3,2,1,0:T(8,128)(2,1)}), bf16[4,2,192,1024]{3,2,1,0:T(8,128)(2,1)}, u32[]{:S(2)}, u32[]{:S(2)}) %all-to-all-start.1) | async-done | bytes 3145760 | tf_op jit(solution)/shard_map/all_to_all | solution.py:253
  166.2 3.7 %fusion.5 = f32[512,1024]{1,0:T(8,128)S(1)} fusion(bf16[1536,1024]{1,0:T(8,128)(2,1)} %bitcast.24, s32[512]{0:T(512)S(1)} %copy-done.15), kind=kOutput, calls=%fused_computation.15 | convolution fusion | flops 1611399168 | bytes 5244928 | tf_op jit(solution)/shard_map/dot_general | solution.py:263
  169.9 4.8 %add_convert_fusion = bf16[512,1024]{1,0:T(8,128)(2,1)} fusion(f32[512,1024]{1,0:T(8,128)S(1)} %fusion.5, bf16[1536,1024]{1,0:T(8,128)(2,1)} %bitcast.24, s32[512]{0:T(512)S(1)} %copy-done.14, f32[512]{0:T(512)S(1)} %bitcast.95, f32[512]{0:T(512)S(1)} %bitcast.94), kind=kOutput, calls=%fused_computation.52 | convolution fusion | flops 1613496320 | bytes 6297600 | tf_op jit(solution)/shard_map/dot_general | solution.py:263
  174.8 27.9 %reduce-scatter.5.cloned.1.call-done = bf16[512,256]{1,0:T(8,128)(2,1)} async-done(((bf16[512,1024]{1,0:T(8,128)(2,1)}), bf16[512,256]{1,0:T(8,128)(2,1)}) %reduce-scatter.5.cloned.1.call-update) | async-done | bytes 262160 | tf_op jit(solution)/shard_map/reduce_scatter | solution.py:267
  (67 shorter events, 6.0 us)
Async XLA Ops:
  7.2 105.0 %copy-start = (bf16[256,2048]{1,0:T(8,128)(2,1)S(1)}, bf16[256,2048]{1,0:T(8,128)(2,1)}, u32[]{:S(2)}) copy-start(bf16[256,2048]{1,0:T(8,128)(2,1)} %param.26) | copy-start | bytes 3145732
  7.2 5.7 %copy-start.6 = (f32[512]{0:T(512)S(1)}, f32[512]{0:T(512)}, u32[]{:S(2)}) copy-start(f32[512]{0:T(512)} %param.21) | copy-start | bytes 6148
  7.2 7.0 %copy-start.11 = (bf16[512,32]{0,1:T(8,128)(2,1)S(1)}, bf16[512,32]{0,1:T(8,128)(2,1)}, u32[]{:S(2)}) copy-start(bf16[512,32]{0,1:T(8,128)(2,1)} %param.19) | copy-start | bytes 98308
  7.2 8.1 %copy-start.1 = (bf16[512,2048]{1,0:T(8,128)(2,1)S(1)}, bf16[512,2048]{1,0:T(8,128)(2,1)}, u32[]{:S(2)}) copy-start(bf16[512,2048]{1,0:T(8,128)(2,1)} %param.27) | copy-start | bytes 6291460
  7.2 57.2 %all-gather.2.cloned.1.call-start = ((), (), s32[]{:S(2)}) async-start(), calls=%async_computation.4 | async-start | bytes 1474560 | tf_op jit(solution)/shard_map/all_gather | solution.py:195
  15.3 3.0 %copy-start.5 = (f32[2048]{0:T(1024)S(1)}, f32[2048]{0:T(1024)}, u32[]{:S(2)}) copy-start(f32[2048]{0:T(1024)} %param.28) | copy-start | bytes 24580
  17.8 2.5 %copy-start.3 = (s32[512,2]{0,1:T(2,128)S(1)}, s32[512,2]{0,1:T(2,128)}, u32[]{:S(2)}) copy-start(s32[512,2]{0,1:T(2,128)} %param.29) | copy-start | bytes 12292
  25.0 5.3 %copy-start.2 = (bf16[512,1024]{1,0:T(8,128)(2,1)S(1)}, bf16[512,1024]{1,0:T(8,128)(2,1)}, u32[]{:S(2)}) copy-start(bf16[512,1024]{1,0:T(8,128)(2,1)} %param.17) | copy-start | bytes 3145732
  25.0 5.6 %copy-start.9 = (bf16[1024,128]{1,0:T(8,128)(2,1)S(1)}, bf16[1024,128]{1,0:T(8,128)(2,1)}, u32[]{:S(2)}) copy-start(bf16[1024,128]{1,0:T(8,128)(2,1)} %param.23) | copy-start | bytes 786436
  25.0 5.6 %copy-start.12 = (f32[1024]{0:T(1024)S(1)}, f32[1024]{0:T(1024)}, u32[]{:S(2)}) copy-start(f32[1024]{0:T(1024)} %param.20) | copy-start | bytes 12292
  25.0 60.4 %all-to-all-start = ((bf16[4,2,192,1024]{3,2,1,0:T(8,128)(2,1)}), bf16[4,2,192,1024]{3,2,1,0:T(8,128)(2,1)}, u32[]{:S(2)}, u32[]{:S(2)}) async-start(bf16[4,2,192,1024]{3,2,1,0:T(8,128)(2,1)} %bitcast.92), calls=%async_computation | async-start | bytes 6291456 | tf_op jit(solution)/shard_map/all_to_all | solution.py:210
  30.4 144.4 %reduce-scatter.3.cloned.1.call-start = ((), (), s32[]{:S(2)}) async-start(), calls=%async_computation.5 | async-start | bytes 2359296 | tf_op jit(solution)/shard_map/reduce_scatter | solution.py:225
  65.7 5.0 %collective-permute-start = (bf16[2048,256]{0,1:T(8,128)(2,1)S(1)}, bf16[2048,256]{0,1:T(8,128)(2,1)}, u32[]{:S(2)}, u32[]{:S(2)}) collective-permute-start(bf16[2048,256]{0,1:T(8,128)(2,1)S(1)} %slice.28), channel_id=1, source_target_pairs={{0,1},{1,0},{2,3},{3,2},{4,5},{5,4},{6,7},{7,6},{8,9},{9,8},{10,11... | collective-permute-start | bytes 3145736 | tf_op jit(solution)/shard_map/ppermute | solution.py:104
  70.7 2.6 %copy-start.10 = (bf16[512,256]{1,0:T(8,128)(2,1)S(1)}, bf16[512,256]{1,0:T(8,128)(2,1)}, u32[]{:S(2)}) copy-start(bf16[512,256]{1,0:T(8,128)(2,1)} %param.25) | copy-start | bytes 786436
  89.4 11.5 %collective-permute-start.1 = (bf16[4,2,192,1024]{3,2,0,1:T(8,128)(2,1)}, bf16[4,2,192,1024]{3,2,0,1:T(8,128)(2,1)}, u32[]{:S(2)}, u32[]{:S(2)}) collective-permute-start(bf16[4,2,192,1024]{3,2,0,1:T(8,128)(2,1)} %copy.28), channel_id=1, source_target_pairs={{0,1},{1,0},{2,3},{3,2},{4,5},{5,4},{6,7},{7,6},{8,9},{9,8},{10,11... | collective-permute-start | bytes 9437192 | tf_op jit(solution)/shard_map/ppermute | solution.py:104
  89.9 3.5 %copy-start.8 = (bf16[2,2048,512]{2,1,0:T(8,128)(2,1)S(1)}, bf16[2,2048,512]{2,1,0:T(8,128)(2,1)}, u32[]{:S(2)}) copy-start(bf16[2,2048,512]{2,1,0:T(8,128)(2,1)} %param.32) | copy-start | bytes 12582916
  93.4 3.8 %copy-start.7 = (bf16[2,2048,512]{2,1,0:T(8,128)(2,1)S(1)}, bf16[2,2048,512]{2,1,0:T(8,128)(2,1)}, u32[]{:S(2)}) copy-start(bf16[2,2048,512]{2,1,0:T(8,128)(2,1)} %param.31) | copy-start | bytes 12582916
  108.9 3.2 %copy-start.13 = (bf16[4,2,192,512]{3,2,0,1:T(8,128)(2,1)}, bf16[4,2,192,512]{3,2,0,1:T(8,128)(2,1)S(1)}, u32[]{:S(2)}) copy-start(bf16[4,2,192,512]{3,2,0,1:T(8,128)(2,1)S(1)} %fusion.1) | copy-start | bytes 4718596
  112.1 6.0 %collective-permute-start.2 = (bf16[4,2,192,1024]{3,2,0,1:T(8,128)(2,1)}, bf16[4,2,192,1024]{3,2,0,1:T(8,128)(2,1)}, u32[]{:S(2)}, u32[]{:S(2)}) collective-permute-start(bf16[4,2,192,1024]{3,2,0,1:T(8,128)(2,1)} %convert_bitcast_fusion), channel_id=1, source_target_pairs={{0,1},{1,0},{2,3},{3,2},{4,5},{5,4},{6,7},{7,6},{8,9},{9,8},{10,11... | collective-permute-start | bytes 9437192 | tf_op jit(solution)/shard_map/ppermute | solution.py:104
  124.6 4.9 %copy-start.4 = (f32[512,2]{0,1:T(2,128)S(1)}, f32[512,2]{0,1:T(2,128)}, u32[]{:S(2)}) copy-start(f32[512,2]{0,1:T(2,128)} %param.30) | copy-start | bytes 12292
  124.7 41.5 %copy-start.15 = (s32[512]{0:T(512)S(1)}, s32[512]{0:T(512)}, u32[]{:S(2)}) copy-start(s32[512]{0:T(512)} %get-tuple-element.11) | copy-start | bytes 6148
  124.7 41.5 %all-to-all-start.1 = ((bf16[4,2,192,1024]{3,2,1,0:T(8,128)(2,1)}), bf16[4,2,192,1024]{3,2,1,0:T(8,128)(2,1)}, u32[]{:S(2)}, u32[]{:S(2)}) async-start(bf16[4,2,192,1024]{3,2,1,0:T(8,128)(2,1)} %copy.31), calls=%async_computation.2 | async-start | bytes 6291456 | tf_op jit(solution)/shard_map/all_to_all | solution.py:253
  129.5 73.3 %reduce-scatter.5.cloned.1.call-start = ((), (), s32[]{:S(2)}) async-start(), calls=%async_computation.6 | async-start | bytes 1310720 | tf_op jit(solution)/shard_map/reduce_scatter | solution.py:267
  166.2 3.7 %copy-start.14 = (s32[512]{0:T(512)S(1)}, s32[512]{0:T(512)}, u32[]{:S(2)}) copy-start(s32[512]{0:T(512)} %get-tuple-element.10) | copy-start | bytes 6148
Sparse Core Ops, SparseCore 0:
  15.4 49.0 all-gather.1
  114.3 35.7 reduce-scatter.2
  174.9 27.7 reduce-scatter.4
